TPU v7x, 32 devices: a whole 2x2x4 slice. The times are simulated.
32 devices in a mesh: sp: 8 (over z, x), tp: 4 (over y, core).
Axes of the slice: x: 2, y: 2, z: 4, core: 2. Of those that a mesh axis runs over, the one named last changes fastest.
Arguments:
- queries: bfloat16 [5120, 2048], P('sp', 'tp'), may hold values from -164 to 164
- keys: bfloat16 [5120, 512], P('sp', 'tp'), may hold values from -6 to 6
- values: bfloat16 [5120, 512], P('sp', 'tp'), may hold values from -6 to 6
- sink: float32 [32], P('tp'), may hold values from 4 to 8
- stream: bfloat16 [5120, 2048], P(('sp', 'tp')), may hold values from -6 to 6
- out_weight: bfloat16 [2048, 2048], P('tp'), may hold values from -0.5390625 to 0.5390625
- norm_gain: float32 [2048], replicated, may hold values from 0.1 to 1.9
- gate_weight: bfloat16 [2048, 5632], P('sp', 'tp'), may hold values from -0.125 to 0.125
- up_weight: bfloat16 [2048, 5632], P('sp', 'tp'), may hold values from -0.125 to 0.125
- down_weight: bfloat16 [5632, 2048], P('tp', 'sp'), may hold values from -0.23925781 to 0.23925781
Outputs:
- result: bfloat16 [5120, 2048], P(('sp', 'tp'))
All inputs are finite; a program needn't handle non-finite values.
Results may differ from a plain program's by a relative error of at most 0.019.
Values may be sent and summed in bfloat16 or wider, within the bound.
A program may use at most 128 MiB of HBM per device.

v0:
```python
import jax
import jax.numpy as jnp
from jax import lax
from jax.sharding import PartitionSpec as P

HEAD = 64
WINDOW = 128


def padded_2(cells, sides, width):
    for axis, dim in sides:
        count = lax.axis_size(axis)
        ends = count - 1
        head = lax.slice_in_dim(cells, 0, width, axis=dim)
        tail = lax.slice_in_dim(cells, cells.shape[dim] - width, cells.shape[dim], axis=dim)
        cells = jnp.concatenate(
            [
                lax.ppermute(tail, axis, [(i, (i + 1) % count) for i in range(ends)]),
                cells,
                lax.ppermute(head, axis, [((i + 1) % count, i) for i in range(ends)]),
            ],
            axis=dim,
        )
    return cells


def rotary(block, start):
    length = block.shape[0]
    middle = HEAD // 2
    inverse = 1.0 / 10000.0 ** (jnp.arange(0, HEAD, 2, dtype=jnp.float32) / HEAD)
    places = (start + jnp.arange(length, dtype=jnp.int32)).astype(jnp.float32)
    angles = places[:, None, None] * inverse[None, None, :]
    cosine_table = jnp.cos(angles)
    sine_table = jnp.sin(angles)
    pieces = block.astype(jnp.float32).reshape(length, -1, HEAD)
    leading = pieces[..., :middle]
    trailing = pieces[..., middle:]
    turned = jnp.concatenate(
        [
            leading * cosine_table - trailing * sine_table,
            trailing * cosine_table + leading * sine_table,
        ],
        -1,
    )
    return turned.reshape(length, -1).astype(jnp.bfloat16)


def window_attend(queries, keys, values, sink):
    rows_here = queries.shape[0]
    start = lax.axis_index("sp") * rows_here
    length = lax.axis_size("sp") * rows_here
    blocks = rows_here // WINDOW
    kv_width = keys.shape[1]
    kv_count = kv_width // HEAD
    head_count = queries.shape[1] // HEAD
    group = head_count // kv_count
    turned_q = rotary(queries, start)
    turned_k = rotary(keys, start)
    paired = jnp.concatenate([turned_k, values], 1)
    padded = padded_2(paired, (("sp", 0),), WINDOW)
    framed = padded.reshape(blocks + 2, WINDOW, 2 * kv_width)
    banded = jnp.concatenate([framed[:-2], framed[1:-1], framed[2:]], axis=1)
    key_band = banded[..., :kv_width].reshape(blocks, 3 * WINDOW, kv_count, HEAD)
    value_band = banded[..., kv_width:].reshape(blocks, 3 * WINDOW, kv_count, HEAD)
    query_blocks = turned_q.reshape(blocks, WINDOW, kv_count, group, HEAD)
    scores = jnp.einsum(
        "nqkgd,nskd->nkgqs", query_blocks, key_band, preferred_element_type=jnp.float32
    ) * HEAD ** (-0.5)
    query_place = (
        start + jnp.arange(blocks)[:, None, None] * WINDOW + jnp.arange(WINDOW)[None, :, None]
    )
    key_place = (
        start
        + jnp.arange(blocks)[:, None, None] * WINDOW
        - WINDOW
        + jnp.arange(3 * WINDOW)[None, None, :]
    )
    valid = (jnp.abs(key_place - query_place) <= WINDOW) & (key_place >= 0) & (key_place < length)
    scores = jnp.where(valid[:, None, None], scores, -jnp.inf)
    sink_grid = sink.reshape(kv_count, group)[None, :, :, None]
    top = jnp.maximum(jnp.max(scores, -1), sink_grid)
    raised = jnp.exp(scores - top[..., None])
    denom = jnp.sum(raised, -1) + jnp.exp(sink_grid - top)
    weights = (raised / denom[..., None]).astype(jnp.bfloat16)
    output = jnp.einsum(
        "nkgqs,nskd->nqkgd", weights, value_band, preferred_element_type=jnp.float32
    )
    return output.astype(jnp.bfloat16).reshape(rows_here, head_count * HEAD)


def collect_weights(gate_weight, up_weight, down_weight):
    return (
        lax.all_gather(gate_weight, "sp", axis=0, tiled=True),
        lax.all_gather(up_weight, "sp", axis=0, tiled=True),
        lax.all_gather(down_weight, "sp", axis=1, tiled=True),
    )


def local(
    queries, keys, values, sink, stream, out_weight, norm_gain, gate_weight, up_weight, down_weight
):
    attended = window_attend(queries, keys, values, sink)
    gathered = collect_weights(gate_weight, up_weight, down_weight)
    gate_whole, up_whole, down_whole = gathered
    rows = attended
    projected = lax.psum_scatter(
        jnp.dot(rows, out_weight, preferred_element_type=jnp.float32),
        "tp",
        scatter_dimension=0,
        tiled=True,
    )
    mixed = (stream.astype(jnp.float32) + projected).astype(jnp.bfloat16)
    mixed_wide = mixed.astype(jnp.float32)
    scale = lax.rsqrt(jnp.mean(mixed_wide * mixed_wide, -1, keepdims=True) + 1e-06)
    normed = (mixed_wide * scale * norm_gain).astype(jnp.bfloat16)
    piece = lax.all_gather(normed, "tp", axis=0, tiled=True)
    gate = jnp.dot(piece, gate_whole, preferred_element_type=jnp.float32)
    upward = jnp.dot(piece, up_whole, preferred_element_type=jnp.float32)
    hidden = (jax.nn.silu(gate) * upward).astype(jnp.bfloat16)
    rows = hidden
    lowered = lax.psum_scatter(
        jnp.dot(rows, down_whole, preferred_element_type=jnp.float32).astype(jnp.bfloat16),
        "tp",
        scatter_dimension=0,
        tiled=True,
    ).astype(jnp.float32)
    return (mixed_wide + 0.5 * lowered).astype(jnp.bfloat16)


def solution(mesh):
    placed = (
        P("sp", "tp"),
        P("sp", "tp"),
        P("sp", "tp"),
        P("tp"),
        P(("sp", "tp"), None),
        P("tp", None),
        P(),
        P("sp", "tp"),
        P("sp", "tp"),
        P("tp", "sp"),
    )
    return jax.shard_map(
        local, mesh=mesh, in_specs=placed, out_specs=P(("sp", "tp"), None), check_vma=False
    )
```

profile of v0, /device:TPU:0, one launch (start us, length us, event | category | flops | bytes accessed | tf_op | source)
XLA Modules:
  0.0 420.8 jit_solution(13338107045309871906)
XLA Ops:
  7.4 1.2 copy.24
  8.6 1.1 copy.25
  10.9 5.5 %collective-permute-start = (bf16[128,256]{0,1:T(8,128)(2,1)}, bf16[128,256]{0,1:T(8,128)(2,1)}, u32[]{:S(2)}, u32[]{:S(2)}) collective-permute-start(bf16[128,256]{0,1:T(8,128)(2,1)} %get-tuple-element.16), channel_id=1, source_target_pairs={{0,4},{4,8},{8,12},{12,16},{16,20},{20,24},{24,28},{1,5},{5,9},{9,... | collective-permute-start | bytes 196616 | tf_op jit(solution)/shard_map/ppermute | solution.py:18
  16.4 1.3 collective-permute-start.1
  17.9 1.4 copy.31
  19.5 1.2 fusion.11
  20.7 0.9 pad_maximum_fusion.1
  21.6 1.8 convert_element_type.55
  23.4 1.3 max.17
  24.8 2.1 pad_maximum_fusion.5
  26.8 1.9 copy.26
  28.7 1.9 copy.27
  30.6 1.9 copy.28
  32.5 1.2 pad_maximum_fusion
  33.7 1.2 fusion.24
  34.9 2.0 copy.30
  36.9 2.3 fusion.1
  39.3 1.9 fusion
  41.2 1.1 copy-done.1
  42.6 5.4 %fusion.9 = bf16[5,128,2,4,64]{1,4,3,2,0:T(8,128)(2,1)S(1)} fusion(bf16[5,384,2,64,1]{1,3,4,2,0:T(8,128)(2,1)S(1)} %bitcast.59, f32[5,2,384,128,4]{3,2,4,1,0:T(8,128)} %copy-done.1, f32[5,2,4,128]{3,2,1,0:T(4,128)S(1)} %exponential_add_fusion, f32[5,2,4,128]{3,2,1,0:T(4,128)S(1)} %broadcast_maximum_fusion, pred[5,128,384]{1,2,0:T(8,128)(4,1)S(1)} %fusion.11), kind=kOutput, calls=%fused_computation.18 | convolution fusion | flops 261816320 | bytes 9297920 | tf_op jit(solution)/shard_map/nkgqs,nskd->nqkgd/dot_general | solution.py:85
  48.5 4.0 fusion.12
  53.2 53.3 %reduce-scatter.3.cloned.1.call-done = f32[160,2048]{1,0:T(8,128)} async-done(((f32[640,2048]{1,0:T(8,128)}), f32[160,2048]{1,0:T(8,128)}) %reduce-scatter.3.cloned.1.call-update) | async-done | bytes 1310736 | tf_op jit(solution)/shard_map/reduce_scatter | solution.py:106
  106.4 1.6 fusion.5
  108.0 1.1 fusion.7
  110.7 39.1 %all-gather.7.cloned.1.call-done = bf16[2048,1408]{1,0:T(8,128)(2,1)} async-done(((bf16[256,1408]{1,0:T(8,128)(2,1)}), bf16[2048,1408]{1,0:T(8,128)(2,1)}) %all-gather.7.cloned.1.call-update) | async-done | bytes 5767184 | tf_op jit(solution)/shard_map/all_gather | solution.py:93
  149.8 25.0 %all-gather.5.cloned.1.call-done = bf16[640,2048]{1,0:T(8,128)(2,1)} async-done(((bf16[160,2048]{1,0:T(8,128)(2,1)}), bf16[640,2048]{1,0:T(8,128)(2,1)}) %all-gather.5.cloned.1.call-update) | async-done | bytes 2621456 | tf_op jit(solution)/shard_map/all_gather | solution.py:116
  174.8 9.4 %fusion.25 = f32[640,1408]{1,0:T(8,128)} fusion(bf16[640,2048]{1,0:T(8,128)(2,1)} %all-gather.5.cloned.1.call-done, bf16[2048,1408]{1,0:T(8,128)(2,1)} %all-gather.7.cloned.1.call-done), kind=kOutput, calls=%fused_computation.62 | convolution fusion | flops 3690987520 | bytes 11993088 | tf_op jit(solution)/shard_map/dot_general | solution.py:117
  184.2 85.4 %all-gather.11.cloned.1.call-done = bf16[1408,2048]{1,0:T(8,128)(2,1)} async-done(((bf16[1408,256]{1,0:T(8,128)(2,1)}), bf16[1408,2048]{1,0:T(8,128)(2,1)}) %all-gather.11.cloned.1.call-update) | async-done | bytes 5767184 | tf_op jit(solution)/shard_map/all_gather | solution.py:95
  269.6 92.5 %all-gather.9.cloned.1.call-done = bf16[2048,1408]{1,0:T(8,128)(2,1)} async-done(((bf16[256,1408]{1,0:T(8,128)(2,1)}), bf16[2048,1408]{1,0:T(8,128)(2,1)}) %all-gather.9.cloned.1.call-update) | async-done | bytes 5767184 | tf_op jit(solution)/shard_map/all_gather | solution.py:94
  362.1 16.1 %convolution_convert_fusion = bf16[640,2048]{1,0:T(8,128)(2,1)} fusion(bf16[1408,2048]{1,0:T(8,128)(2,1)} %all-gather.11.cloned.1.call-done, bf16[640,2048]{1,0:T(8,128)(2,1)} %all-gather.5.cloned.1.call-done, bf16[2048,1408]{1,0:T(8,128)(2,1)} %all-gather.9.cloned.1.call-done, f32[640,1408]{1,0:T(8,128)} %fusion.25), kind=kOutput, calls=%fused_computation.8 | convolution fusion | flops 7388692480 | bytes 20381696 | tf_op jit(solution)/shard_map/dot_general | solution.py:122
  378.3 32.8 %reduce-scatter.5.cloned.1.call-done = bf16[160,2048]{1,0:T(8,128)(2,1)} async-done(((bf16[640,2048]{1,0:T(8,128)(2,1)}), bf16[160,2048]{1,0:T(8,128)(2,1)}) %reduce-scatter.5.cloned.1.call-update) | async-done | bytes 655376 | tf_op jit(solution)/shard_map/reduce_scatter | solution.py:121
  411.1 2.1 fusion.8
  (45 shorter events, 4.8 us)
Async XLA Ops:
  7.4 41.2 %copy-start = (bf16[512,2048]{1,0:T(8,128)(2,1)S(1)}, bf16[512,2048]{1,0:T(8,128)(2,1)}, u32[]{:S(2)}) copy-start(bf16[512,2048]{1,0:T(8,128)(2,1)} %param.15) | copy-start | bytes 6291460
  7.4 99.1 %reduce-scatter.3.cloned.1.call-start = ((), (), s32[]{:S(2)}) async-start(), calls=%async_computation.2 | async-start | bytes 6553600 | tf_op jit(solution)/shard_map/reduce_scatter | solution.py:106
  10.2 7.6 %copy-start.3 = (bf16[640,2,64]{0,2,1:T(8,128)(2,1)}, bf16[640,2,64]{0,2,1:T(8,128)(2,1)S(1)}, u32[]{:S(2)}) copy-start(bf16[640,2,64]{0,2,1:T(8,128)(2,1)S(1)} %pad_maximum_fusion.7) | copy-start | bytes 491524
  10.9 13.9 %collective-permute-start = (bf16[128,256]{0,1:T(8,128)(2,1)}, bf16[128,256]{0,1:T(8,128)(2,1)}, u32[]{:S(2)}, u32[]{:S(2)}) collective-permute-start(bf16[128,256]{0,1:T(8,128)(2,1)} %get-tuple-element.16), channel_id=1, source_target_pairs={{0,4},{4,8},{8,12},{12,16},{16,20},{20,24},{24,28},{1,5},{5,9},{9,... | collective-permute-start | bytes 196616 | tf_op jit(solution)/shard_map/ppermute | solution.py:18
  16.4 8.4 %collective-permute-start.1 = (bf16[128,256]{0,1:T(8,128)(2,1)}, bf16[128,256]{0,1:T(8,128)(2,1)}, u32[]{:S(2)}, u32[]{:S(2)}) collective-permute-start(bf16[128,256]{0,1:T(8,128)(2,1)} %get-tuple-element.17), channel_id=1, source_target_pairs={{4,0},{8,4},{12,8},{16,12},{20,16},{24,20},{28,24},{5,1},{9,5},{13... | collective-permute-start | bytes 196616 | tf_op jit(solution)/shard_map/ppermute | solution.py:20
  36.9 2.3 copy-start.6
  39.2 3.1 copy-start.1
  39.3 3.0 copy-start.2
  52.5 53.9 %copy-start.4 = (bf16[160,2048]{1,0:T(8,128)(2,1)S(1)}, bf16[160,2048]{1,0:T(8,128)(2,1)}, u32[]{:S(2)}) copy-start(bf16[160,2048]{1,0:T(8,128)(2,1)} %param.14) | copy-start | bytes 1966084
  52.5 55.5 %copy-start.5 = (f32[2048]{0:T(1024)S(1)}, f32[2048]{0:T(1024)}, u32[]{:S(2)}) copy-start(f32[2048]{0:T(1024)} %param.16) | copy-start | bytes 24580
  52.5 97.2 %all-gather.7.cloned.1.call-start = ((), (), s32[]{:S(2)}) async-start(), calls=%async_computation.4 | async-start | bytes 6488064 | tf_op jit(solution)/shard_map/all_gather | solution.py:93
  53.1 121.7 %all-gather.5.cloned.1.call-start = ((), (), s32[]{:S(2)}) async-start(), calls=%async_computation.3 | async-start | bytes 3276800 | tf_op jit(solution)/shard_map/all_gather | solution.py:116
  109.1 160.5 %all-gather.11.cloned.1.call-start = ((), (), s32[]{:S(2)}) async-start(), calls=%async_computation.6 | async-start | bytes 6488064 | tf_op jit(solution)/shard_map/all_gather | solution.py:95
  109.7 252.4 %all-gather.9.cloned.1.call-start = ((), (), s32[]{:S(2)}) async-start(), calls=%async_computation.5 | async-start | bytes 6488064 | tf_op jit(solution)/shard_map/all_gather | solution.py:94
  110.4 300.6 %reduce-scatter.5.cloned.1.call-start = ((), (), s32[]{:S(2)}) async-start(), calls=%async_computation.7 | async-start | bytes 3276800 | tf_op jit(solution)/shard_map/reduce_scatter | solution.py:121
Sparse Core Ops, SparseCore 0:
  52.7 53.7 reduce-scatter.2
  378.4 32.6 reduce-scatter.4
Sparse Core Ops, SparseCore 1:
  55.2 94.5 all-gather.6
  151.2 23.5 all-gather.4
  176.7 92.8 all-gather.10
  271.8 90.3 all-gather.8
where the time goes:
time: 421 us
  waiting for transfers between devices  330 us (78%)
  matrix products  37.2 us (9%)
  local copies, waits for them, and re-layouts  17.4 us (4%)
  between operations  15.2 us (4%)
  other arithmetic  13.9 us (3%)
  starting transfers between devices  7.16 us (2%)
    all_gather x1, waiting for transfers between devices, collect_weights(): lax.all_gather(up_weight, 'sp', axis=0, tiled=True)  92.5 us
    all_gather x1, waiting for transfers between devices, collect_weights(): lax.all_gather(down_weight, 'sp', axis=1, tiled=True)  85.4 us
    reduce_scatter x1, waiting for transfers between devices, local(): lax.psum_scatter(jnp.dot(rows, out_weight, preferred_element_type=jnp.flo...  53.3 us
    all_gather x1, waiting for transfers between devices, collect_weights(): lax.all_gather(gate_weight, 'sp', axis=0, tiled=True)  39.1 us
    reduce_scatter x1, waiting for transfers between devices, local(): lax.psum_scatter(jnp.dot(rows, down_whole, preferred_element_type=jnp.flo...  32.8 us
    all_gather x1, waiting for transfers between devices, local(): piece = lax.all_gather(normed, 'tp', axis=0, tiled=True)  25 us
    dot_general x1, matrix products, local(): jnp.dot(rows, down_whole, preferred_element_type=jnp.float32)  16.1 us
    dot_general x1, matrix products, local(): gate = jnp.dot(piece, gate_whole, preferred_element_type=jnp.float32)  9.43 us
  transfers between devices with their start and end apart: 8, of which 6 were waited for; matrix products, arithmetic and copies ran while one was open for 5% of the time, Pallas kernels for 0%

commit v1 on v0

--- a/solution.py
+++ b/solution.py
@@ -2,9 +2,23 @@
 import jax.numpy as jnp
 from jax import lax
 from jax.sharding import PartitionSpec as P
+from jax.lax import axis_index, axis_size, ppermute
 
 HEAD = 64
 WINDOW = 128
+
+
+def create_levels_all_up(field, d0=0):
+    n_chips = axis_size("tp")
+    seen = tuple(((k, (k + 1) % n_chips) for k in range(n_chips)))
+
+    def _resolve_lane(arr_now):
+        if len(arr_now) == n_chips:
+            return arr_now
+        return _resolve_lane([ppermute(arr_now[0], "tp", seen), *arr_now])
+
+    block_now = jnp.concatenate(_resolve_lane([field]), axis=d0)
+    return jnp.roll(block_now, shift=(axis_index("tp") + 1) * field.shape[d0], axis=d0)
 
 
 def padded_2(cells, sides, width):
@@ -113,7 +127,7 @@
     mixed_wide = mixed.astype(jnp.float32)
     scale = lax.rsqrt(jnp.mean(mixed_wide * mixed_wide, -1, keepdims=True) + 1e-06)
     normed = (mixed_wide * scale * norm_gain).astype(jnp.bfloat16)
-    piece = lax.all_gather(normed, "tp", axis=0, tiled=True)
+    piece = create_levels_all_up(normed)
     gate = jnp.dot(piece, gate_whole, preferred_element_type=jnp.float32)
     upward = jnp.dot(piece, up_whole, preferred_element_type=jnp.float32)
     hidden = (jax.nn.silu(gate) * upward).astype(jnp.bfloat16)

time: 421 us -> 397 us (0.943)
  waiting for transfers between devices: 330 us -> 292 us
  local copies, waits for them, and re-layouts: 17.4 us -> 29.1 us
    all_gather x1, waiting for transfers between devices: 39.1 us -> 0.01 us  [collect_weights(): lax.all_gather(gate_weight, 'sp', axis=0, tiled=True)]
    ppermute x0 -> x3, waiting for transfers between devices: none -> 30.4 us  [_resolve_lane(): return _resolve_lane([ppermute(arr_now[0], 'tp', seen), *arr_now])]
    all_gather x1 -> x0, waiting for transfers between devices: 25 us -> none  [local(): piece = lax.all_gather(normed, 'tp', axis=0, tiled=True)]
    unnamed x17 -> x23, local copies, waits for them, and re-layouts: 4.74 us -> 16.4 us
    all_gather x1, waiting for transfers between devices: 92.5 us -> 81.7 us  [collect_weights(): lax.all_gather(up_weight, 'sp', axis=0, tiled=True)]
    all_gather x1, waiting for transfers between devices: 85.4 us -> 93 us  [collect_weights(): lax.all_gather(down_weight, 'sp', axis=1, tiled=True)]
  transfers between devices with their start and end apart: 8 -> 10, of which waited for: 6 -> 7; matrix products, arithmetic and copies ran while one was open for 5% -> 8% of each run, Pallas kernels for 0% -> 0%
where the time goes in v1:
time: 397 us; the launch traced here: 396 us
  waiting for transfers between devices  292 us (74%)
  matrix products  37.4 us (9%)
  local copies, waits for them, and re-layouts  29.1 us (7%)
  other arithmetic  15.2 us (4%)
  between operations  15.2 us (4%)
  starting transfers between devices  7.18 us (2%)
    all_gather x1, waiting for transfers between devices, collect_weights(): lax.all_gather(down_weight, 'sp', axis=1, tiled=True)  93 us
    all_gather x1, waiting for transfers between devices, collect_weights(): lax.all_gather(up_weight, 'sp', axis=0, tiled=True)  81.7 us
    reduce_scatter x1, waiting for transfers between devices, local(): lax.psum_scatter(jnp.dot(rows, out_weight, preferred_element_type=jnp.flo...  52.1 us
    reduce_scatter x1, waiting for transfers between devices, local(): lax.psum_scatter(jnp.dot(rows, down_whole, preferred_element_type=jnp.flo...  32.8 us
    ppermute x3, waiting for transfers between devices, _resolve_lane(): return _resolve_lane([ppermute(arr_now[0], 'tp', seen), *arr_now])  30.4 us
    unnamed x23, local copies, waits for them, and re-layouts  16.4 us
    dot_general x1, matrix products, local(): jnp.dot(rows, down_whole, preferred_element_type=jnp.float32)  16.3 us
    dot_general x1, matrix products, local(): gate = jnp.dot(piece, gate_whole, preferred_element_type=jnp.float32)  9.5 us
  transfers between devices with their start and end apart: 10, of which 7 were waited for; matrix products, arithmetic and copies ran while one was open for 8% of the time, Pallas kernels for 0%

profile of v1, /device:TPU:0, one launch (start us, length us, event | category | flops | bytes accessed | tf_op | source)
XLA Modules:
  0.0 395.7 jit_solution(17871419639877126608)
XLA Ops:
  7.4 1.2 copy.24
  10.9 5.5 %collective-permute-start = (bf16[128,256]{0,1:T(8,128)(2,1)}, bf16[128,256]{0,1:T(8,128)(2,1)}, u32[]{:S(2)}, u32[]{:S(2)}) collective-permute-start(bf16[128,256]{0,1:T(8,128)(2,1)} %get-tuple-element.16), channel_id=1, source_target_pairs={{0,4},{4,8},{8,12},{12,16},{16,20},{20,24},{24,28},{1,5},{5,9},{9,... | collective-permute-start | bytes 196616 | tf_op jit(solution)/shard_map/ppermute | solution.py:32
  16.4 1.3 collective-permute-start.1
  17.9 1.4 copy.31
  21.6 1.8 convert_element_type.55
  23.4 1.3 max.17
  24.8 2.1 pad_maximum_fusion.5
  26.8 1.9 copy.26
  28.7 1.9 copy.27
  30.6 1.9 copy.28
  32.5 1.2 pad_maximum_fusion
  34.9 2.0 copy.30
  36.9 2.3 fusion.1
  39.3 2.9 copy-done.1
  42.3 1.9 fusion
  44.5 5.4 %fusion.14 = bf16[5,128,2,4,64]{1,4,3,2,0:T(8,128)(2,1)S(1)} fusion(bf16[5,384,2,64,1]{1,3,4,2,0:T(8,128)(2,1)S(1)} %bitcast.57, f32[5,2,384,128,4]{3,2,4,1,0:T(8,128)} %copy-done.1, f32[5,2,4,128]{3,2,1,0:T(4,128)S(1)} %exponential_add_fusion, f32[5,2,4,128]{3,2,1,0:T(4,128)S(1)} %broadcast_maximum_fusion, pred[5,128,384]{1,2,0:T(8,128)(4,1)S(1)} %fusion.16), kind=kOutput, calls=%fused_computation.21 | convolution fusion | flops 261816320 | bytes 9297920 | tf_op jit(solution)/shard_map/nkgqs,nskd->nqkgd/dot_general | solution.py:99
  50.5 3.9 fusion.19
  56.2 52.1 %reduce-scatter.3.cloned.1.call-done = f32[160,2048]{1,0:T(8,128)} async-done(((f32[640,2048]{1,0:T(8,128)}), f32[160,2048]{1,0:T(8,128)}) %reduce-scatter.3.cloned.1.call-update) | async-done | bytes 1310736 | tf_op jit(solution)/shard_map/reduce_scatter | solution.py:120
  108.3 1.6 fusion.10
  110.4 10.0 %collective-permute-done.2 = bf16[160,2048]{1,0:T(8,128)(2,1)S(1)} collective-permute-done((bf16[160,2048]{1,0:T(8,128)(2,1)S(1)}, bf16[160,2048]{1,0:T(8,128)(2,1)S(1)}, u32[]{:S(2)}, u32[]{:S(2)}) %collective-permute-start.2) | collective-permute-done | bytes 655392 | tf_op jit(solution)/shard_map/ppermute | solution.py:18
  120.4 10.1 %collective-permute-done.3 = bf16[160,2048]{1,0:T(8,128)(2,1)} collective-permute-done((bf16[160,2048]{1,0:T(8,128)(2,1)S(1)}, bf16[160,2048]{1,0:T(8,128)(2,1)}, u32[]{:S(2)}, u32[]{:S(2)}) %collective-permute-start.3) | collective-permute-done | bytes 655392 | tf_op jit(solution)/shard_map/ppermute | solution.py:18
  130.5 10.3 %collective-permute-done.4 = bf16[160,2048]{1,0:T(8,128)(2,1)} collective-permute-done((bf16[160,2048]{1,0:T(8,128)(2,1)}, bf16[160,2048]{1,0:T(8,128)(2,1)}, u32[]{:S(2)}, u32[]{:S(2)}) %collective-permute-start.4) | collective-permute-done | bytes 655392 | tf_op jit(solution)/shard_map/ppermute | solution.py:18
  140.8 2.0 constant_dynamic-update-slice_fusion.7
  142.8 2.0 constant_dynamic-update-slice_fusion.6
  146.8 2.0 constant_dynamic-update-slice_fusion.3
  148.8 2.0 constant_dynamic-update-slice_fusion.2
  152.8 9.5 %fusion.5 = f32[640,1408]{1,0:T(8,128)} fusion(bf16[2048,1408]{1,0:T(8,128)(2,1)} %all-gather.4.cloned.1.call-done, bf16[1280,2048]{1,0:T(8,128)(2,1)} %constant_dynamic-update-slice_fusion, s32[]{:T(128)S(6)} %select_n.19), kind=kOutput, calls=%fused_computation.10 | convolution fusion | flops 3690987520 | bytes 11993092 | tf_op jit(solution)/shard_map/dot_general | solution.py:131
  162.3 81.7 %all-gather.6.cloned.1.call-done = bf16[2048,1408]{1,0:T(8,128)(2,1)} async-done(((bf16[256,1408]{1,0:T(8,128)(2,1)}), bf16[2048,1408]{1,0:T(8,128)(2,1)}) %all-gather.6.cloned.1.call-update) | async-done | bytes 5767184 | tf_op jit(solution)/shard_map/all_gather | solution.py:108
  244.0 93.0 %all-gather.8.cloned.1.call-done = bf16[1408,2048]{1,0:T(8,128)(2,1)} async-done(((bf16[1408,256]{1,0:T(8,128)(2,1)}), bf16[1408,2048]{1,0:T(8,128)(2,1)}) %all-gather.8.cloned.1.call-update) | async-done | bytes 5767184 | tf_op jit(solution)/shard_map/all_gather | solution.py:109
  336.9 16.3 %convolution_convert_fusion = bf16[640,2048]{1,0:T(8,128)(2,1)} fusion(bf16[1408,2048]{1,0:T(8,128)(2,1)} %all-gather.8.cloned.1.call-done, f32[640,1408]{1,0:T(8,128)} %fusion.5, bf16[2048,1408]{1,0:T(8,128)(2,1)} %all-gather.6.cloned.1.call-done, bf16[1280,2048]{1,0:T(8,128)(2,1)} %constant_dynamic-update-slice_fusion, s32[]{:T(128)S(6)} %select_n.19), kind=kOutput, calls=%fused_computation.7 | convolution fusion | flops 7388692480 | bytes 20381700 | tf_op jit(solution)/shard_map/dot_general | solution.py:136
  353.3 32.8 %reduce-scatter.5.cloned.1.call-done = bf16[160,2048]{1,0:T(8,128)(2,1)} async-done(((bf16[640,2048]{1,0:T(8,128)(2,1)}), bf16[160,2048]{1,0:T(8,128)(2,1)}) %reduce-scatter.5.cloned.1.call-update) | async-done | bytes 655376 | tf_op jit(solution)/shard_map/reduce_scatter | solution.py:135
  386.0 2.1 fusion.13
  (56 shorter events, 13.2 us)
Async XLA Ops:
  7.4 43.1 %copy-start = (bf16[512,2048]{1,0:T(8,128)(2,1)S(1)}, bf16[512,2048]{1,0:T(8,128)(2,1)}, u32[]{:S(2)}) copy-start(bf16[512,2048]{1,0:T(8,128)(2,1)} %param.15) | copy-start | bytes 6291460
  7.4 100.9 %reduce-scatter.3.cloned.1.call-start = ((), (), s32[]{:S(2)}) async-start(), calls=%async_computation.2 | async-start | bytes 6553600 | tf_op jit(solution)/shard_map/reduce_scatter | solution.py:120
  10.2 7.6 %copy-start.3 = (bf16[640,2,64]{0,2,1:T(8,128)(2,1)}, bf16[640,2,64]{0,2,1:T(8,128)(2,1)S(1)}, u32[]{:S(2)}) copy-start(bf16[640,2,64]{0,2,1:T(8,128)(2,1)S(1)} %pad_maximum_fusion.7) | copy-start | bytes 491524
  10.9 13.9 %collective-permute-start = (bf16[128,256]{0,1:T(8,128)(2,1)}, bf16[128,256]{0,1:T(8,128)(2,1)}, u32[]{:S(2)}, u32[]{:S(2)}) collective-permute-start(bf16[128,256]{0,1:T(8,128)(2,1)} %get-tuple-element.16), channel_id=1, source_target_pairs={{0,4},{4,8},{8,12},{12,16},{16,20},{20,24},{24,28},{1,5},{5,9},{9,... | collective-permute-start | bytes 196616 | tf_op jit(solution)/shard_map/ppermute | solution.py:32
  16.4 8.4 %collective-permute-start.1 = (bf16[128,256]{0,1:T(8,128)(2,1)}, bf16[128,256]{0,1:T(8,128)(2,1)}, u32[]{:S(2)}, u32[]{:S(2)}) collective-permute-start(bf16[128,256]{0,1:T(8,128)(2,1)} %get-tuple-element.17), channel_id=1, source_target_pairs={{4,0},{8,4},{12,8},{16,12},{20,16},{24,20},{28,24},{5,1},{9,5},{13... | collective-permute-start | bytes 196616 | tf_op jit(solution)/shard_map/ppermute | solution.py:34
  36.9 2.3 copy-start.6
  39.2 3.1 copy-start.1
  39.2 5.0 %copy-start.2 = (bf16[5,384,128]{2,1,0:T(8,128)(2,1)S(1)}, bf16[5,384,128]{2,1,0:T(8,128)(2,1)}, u32[]{:S(2)}) copy-start(bf16[5,384,128]{2,1,0:T(8,128)(2,1)} %get-tuple-element.10) | copy-start | bytes 1474564
  54.4 54.0 %copy-start.4 = (bf16[160,2048]{1,0:T(8,128)(2,1)S(1)}, bf16[160,2048]{1,0:T(8,128)(2,1)}, u32[]{:S(2)}) copy-start(bf16[160,2048]{1,0:T(8,128)(2,1)} %param.14) | copy-start | bytes 1966084
  54.4 55.6 %copy-start.5 = (f32[2048]{0:T(1024)S(1)}, f32[2048]{0:T(1024)}, u32[]{:S(2)}) copy-start(f32[2048]{0:T(1024)} %param.16) | copy-start | bytes 24580
  54.4 98.4 %all-gather.4.cloned.1.call-start = ((), (), s32[]{:S(2)}) async-start(), calls=%async_computation.3 | async-start | bytes 6488064 | tf_op jit(solution)/shard_map/all_gather | solution.py:107
  55.0 189.0 %all-gather.6.cloned.1.call-start = ((), (), s32[]{:S(2)}) async-start(), calls=%async_computation.4 | async-start | bytes 6488064 | tf_op jit(solution)/shard_map/all_gather | solution.py:108
  55.6 281.4 %all-gather.8.cloned.1.call-start = ((), (), s32[]{:S(2)}) async-start(), calls=%async_computation.5 | async-start | bytes 6488064 | tf_op jit(solution)/shard_map/all_gather | solution.py:109
  56.1 329.9 %reduce-scatter.5.cloned.1.call-start = ((), (), s32[]{:S(2)}) async-start(), calls=%async_computation.6 | async-start | bytes 3276800 | tf_op jit(solution)/shard_map/reduce_scatter | solution.py:135
  110.1 10.2 %collective-permute-start.2 = (bf16[160,2048]{1,0:T(8,128)(2,1)S(1)}, bf16[160,2048]{1,0:T(8,128)(2,1)S(1)}, u32[]{:S(2)}, u32[]{:S(2)}) collective-permute-start(bf16[160,2048]{1,0:T(8,128)(2,1)S(1)} %fusion.12), channel_id=1, source_target_pairs={{0,1},{1,2},{2,3},{3,0},{4,5},{5,6},{6,7},{7,4},{8,9},{9,10},{10,1... | collective-permute-start | bytes 1966088 | tf_op jit(solution)/shard_map/ppermute | solution.py:18
  120.4 10.1 %collective-permute-start.3 = (bf16[160,2048]{1,0:T(8,128)(2,1)S(1)}, bf16[160,2048]{1,0:T(8,128)(2,1)}, u32[]{:S(2)}, u32[]{:S(2)}) collective-permute-start(bf16[160,2048]{1,0:T(8,128)(2,1)S(1)} %collective-permute-done.2), channel_id=1, source_target_pairs={{0,1},{1,2},{2,3},{3,0},{4,5},{5,6},{6,7},{7,4},{8,9},{9,10},{10,1... | collective-permute-start | bytes 1966088 | tf_op jit(solution)/shard_map/ppermute | solution.py:18
  130.5 10.3 %collective-permute-start.4 = (bf16[160,2048]{1,0:T(8,128)(2,1)}, bf16[160,2048]{1,0:T(8,128)(2,1)}, u32[]{:S(2)}, u32[]{:S(2)}) collective-permute-start(bf16[160,2048]{1,0:T(8,128)(2,1)} %collective-permute-done.3), channel_id=1, source_target_pairs={{0,1},{1,2},{2,3},{3,0},{4,5},{5,6},{6,7},{7,4},{8,9},{9,10},{10,1... | collective-permute-start | bytes 1966088 | tf_op jit(solution)/shard_map/ppermute | solution.py:18
Sparse Core Ops, SparseCore 0:
  54.5 53.7 reduce-scatter.2
  353.4 32.6 reduce-scatter.4
Sparse Core Ops, SparseCore 1:
  57.1 94.5 all-gather.3
  153.7 90.2 all-gather.5
  245.9 91.0 all-gather.7
